TPU v7x, 32 devices: a whole 2x2x4 slice. The times are simulated.
32 devices in a mesh: dp: 4 (over y, x), kv: 4 (over z), tp: 2 (over core).
Axes of the slice: x: 2, y: 2, z: 4, core: 2. Of those that a mesh axis runs over, the one named last changes fastest.
Arguments:
- tokens: bfloat16 [32, 4, 2048], P('dp', None, 'kv'), may hold values from -600 to 600
- input_norm_gain: float32 [2048], P('kv'), may hold values from 0.1 to 1.9
- query_projection: bfloat16 [2048, 1024], P('kv', 'tp'), may hold values from -0.125 to 0.125
- key_projection: bfloat16 [2048, 1024], P('kv', 'tp'), may hold values from -0.125 to 0.125
- value_projection: bfloat16 [2048, 1024], P('kv', 'tp'), may hold values from -0.125 to 0.125
- write_strength_weight: bfloat16 [2048, 16], P('kv', 'tp'), may hold values from -0.125 to 0.125
- decay_projection: bfloat16 [2048, 16], P('kv', 'tp'), may hold values from -0.125 to 0.125
- head_decay_rate: float32 [16], P('tp'), may hold values from 0.02 to 0.6
- token_extra_decay: float32 [32, 4, 16], P(('dp', 'kv'), None, 'tp'), may hold values from -0.7 to 0
- accepted: int32 [32], P(('dp', 'kv')), may hold values from 1 to 4
- prior_step_states: float32 [32, 4, 16, 4096], P(('dp', 'kv'), None, 'tp'), may hold values from -4 to 4
- output_norm_gain: float32 [64], replicated, may hold values from 0.1 to 1.9
- output_projection: bfloat16 [1024, 2048], P('tp', 'kv'), may hold values from -0.1875 to 0.1875
Outputs:
- mixed: bfloat16 [32, 4, 2048], P('dp', None, 'kv')
- updated_states: float32 [32, 4, 16, 4096], P(('dp', 'kv'), None, 'tp')
Inputs may be any that keep to these rules, and one draw needn't show every extreme that they name: `accepted`: how many proposals of the previous step each sequence kept; its state after that many is taken up.
All inputs are finite; a program needn't handle non-finite values.
Results may differ from a plain program's by a relative error of at most 0.029.
Values may be sent and summed in bfloat16 or wider, within the bound.
A program may use at most 64 MiB of HBM per device.

v0:
```python
import jax
import jax.numpy as jnp
from jax import lax
from jax.sharding import PartitionSpec as P

D = 2048


epsilon = 1e-06
highest = lax.Precision.HIGHEST


def unit_rows(values):
    return values * lax.rsqrt(jnp.sum(values * values, axis=-1, keepdims=True) + epsilon)


def delta_block(query_heads, key_heads, value_heads, beta_gate, decay_logarithm, start_state):
    proposal_len = query_heads.shape[2]
    cumulative = jnp.cumsum(decay_logarithm, axis=-1)
    spread = cumulative[..., :, None] - cumulative[..., None, :]
    strict = jnp.tril(jnp.ones((proposal_len, proposal_len), bool), -1)
    inclusive = jnp.tril(jnp.ones((proposal_len, proposal_len), bool))
    key_inner = jnp.einsum("nhid,nhjd->nhij", key_heads, key_heads, precision=highest)
    coupling = jnp.where(
        strict, beta_gate[..., :, None] * key_inner * jnp.exp(jnp.where(strict, spread, 0.0)), 0.0
    )
    growth = jnp.exp(cumulative)
    right_w = (beta_gate * growth)[..., None] * key_heads
    right_u = beta_gate[..., None] * value_heads
    solved_w = []
    solved_u = []
    for current in range(proposal_len):
        part_w = right_w[:, :, current]
        part_u = right_u[:, :, current]
        for earlier in range(current):
            factor = coupling[:, :, current, earlier][..., None]
            part_w = part_w - factor * solved_w[earlier]
            part_u = part_u - factor * solved_u[earlier]
        solved_w.append(part_w)
        solved_u.append(part_u)
    weights_w = jnp.stack(solved_w, axis=2)
    weights_u = jnp.stack(solved_u, axis=2)
    corrected = weights_u - jnp.einsum("nhpd,nhde->nhpe", weights_w, start_state, precision=highest)
    within = jnp.where(inclusive, jnp.exp(jnp.where(inclusive, spread, 0.0)), 0.0)
    scores = jnp.einsum("nhid,nhjd->nhij", query_heads, key_heads, precision=highest) * within
    attended = jnp.einsum(
        "nhpd,nhde->nhpe", query_heads * growth[..., None], start_state, precision=highest
    ) + jnp.einsum("nhij,nhje->nhie", scores, corrected, precision=highest)
    states = growth[..., None, None] * start_state[:, :, None] + jnp.einsum(
        "nhtj,nhjd,nhje->nhtde", within, key_heads, corrected, precision=highest
    )
    return (attended, states)


def combine_heads(
    query_logits,
    key_logits,
    value_logits,
    beta_logits,
    decay_logits,
    head_decay_rate,
    token_extra_decay,
    accepted,
    prior_step_states,
    output_norm_gain,
):
    seq_count, proposal_len, head_count = beta_logits.shape
    head_size = query_logits.shape[-1] // head_count

    def by_heads(values):
        return jnp.transpose(
            values.reshape(seq_count, proposal_len, head_count, head_size), (0, 2, 1, 3)
        )

    query_heads = unit_rows(by_heads(jax.nn.silu(query_logits))) * head_size ** (-0.5)
    key_heads = unit_rows(by_heads(jax.nn.silu(key_logits)))
    value_heads = by_heads(jax.nn.silu(value_logits))
    beta_gate = jnp.transpose(jax.nn.sigmoid(beta_logits), (0, 2, 1))
    decay_logarithm = jnp.transpose(
        -head_decay_rate[None, None, :] * jax.nn.softplus(decay_logits) + token_extra_decay,
        (0, 2, 1),
    )
    chosen = jnp.arange(proposal_len, dtype=jnp.int32)[None, :] == (accepted - 1)[:, None]
    picked = jnp.sum(jnp.where(chosen[:, :, None, None], prior_step_states, 0.0), axis=1)
    start_state = picked.reshape(seq_count, head_count, head_size, head_size)
    attended, states = delta_block(
        query_heads, key_heads, value_heads, beta_gate, decay_logarithm, start_state
    )
    inverse_rms = lax.rsqrt(jnp.mean(attended * attended, axis=-1, keepdims=True) + epsilon)
    normalized_rows = (attended * inverse_rms * output_norm_gain).astype(jnp.bfloat16)
    normalized_rows = jnp.transpose(normalized_rows, (0, 2, 1, 3)).reshape(
        seq_count, proposal_len, head_count * head_size
    )
    updated_states = jnp.transpose(states, (0, 2, 1, 3, 4)).reshape(
        seq_count, proposal_len, head_count, head_size * head_size
    )
    return (normalized_rows, updated_states)


def per_device(
    tokens,
    input_norm_gain,
    query_projection,
    key_projection,
    value_projection,
    write_strength_weight,
    decay_projection,
    head_decay_rate,
    token_extra_decay,
    accepted,
    prior_step_states,
    output_norm_gain,
    output_projection,
):
    group_seqs, proposal_len, feature_dev = tokens.shape
    own_seqs = prior_step_states.shape[0]
    own_rows = own_seqs * proposal_len
    token_rows = tokens.reshape(group_seqs * proposal_len, feature_dev).astype(jnp.float32)
    squares = jnp.sum(token_rows * token_rows, axis=1)
    scaled = (token_rows * input_norm_gain[None, :]).astype(jnp.bfloat16)
    part_query = jnp.dot(scaled, query_projection, preferred_element_type=jnp.float32)
    part_key = jnp.dot(scaled, key_projection, preferred_element_type=jnp.float32)
    part_value = jnp.dot(scaled, value_projection, preferred_element_type=jnp.float32)
    part_beta = jnp.dot(scaled, write_strength_weight, preferred_element_type=jnp.float32)
    part_decay = jnp.dot(scaled, decay_projection, preferred_element_type=jnp.float32)
    summed = (
        lax.psum_scatter(part_query, "kv", scatter_dimension=0, tiled=True),
        lax.psum_scatter(part_key, "kv", scatter_dimension=0, tiled=True),
        lax.psum_scatter(part_value, "kv", scatter_dimension=0, tiled=True),
        lax.psum_scatter(part_beta, "kv", scatter_dimension=0, tiled=True),
        lax.psum_scatter(part_decay, "kv", scatter_dimension=0, tiled=True),
        lax.psum_scatter(squares, "kv", scatter_dimension=0, tiled=True),
    )
    query_sum, key_sum, value_sum, beta_sum, decay_sum, square_sum = summed
    inverse = lax.rsqrt(square_sum / D + epsilon)[:, None]

    def own_form(values):
        return (values * inverse).reshape(own_seqs, proposal_len, values.shape[1])

    normalized_rows, updated_states = combine_heads(
        own_form(query_sum),
        own_form(key_sum),
        own_form(value_sum),
        own_form(beta_sum),
        own_form(decay_sum),
        head_decay_rate,
        token_extra_decay,
        accepted,
        prior_step_states,
        output_norm_gain,
    )
    normed_rows = normalized_rows.reshape(own_rows, normalized_rows.shape[2])
    partial_value = jnp.dot(
        lax.all_gather(normed_rows, "kv", axis=0, tiled=True),
        output_projection,
        preferred_element_type=jnp.float32,
    )
    mixed = lax.psum(partial_value.astype(jnp.bfloat16), "tp").astype(jnp.float32)
    mixed = mixed.astype(jnp.bfloat16).reshape(group_seqs, proposal_len, output_projection.shape[1])
    return (mixed, updated_states)


def solution(mesh):
    in_specs = (
        P("dp", None, "kv"),
        P("kv"),
        P("kv", "tp"),
        P("kv", "tp"),
        P("kv", "tp"),
        P("kv", "tp"),
        P("kv", "tp"),
        P("tp"),
        P(("dp", "kv"), None, "tp"),
        P(("dp", "kv")),
        P(("dp", "kv"), None, "tp", None),
        P(),
        P("tp", "kv"),
    )
    out_specs = (P("dp", None, "kv"), P(("dp", "kv"), None, "tp", None))
    return jax.shard_map(
        per_device, mesh=mesh, in_specs=in_specs, out_specs=out_specs, check_vma=False
    )
```

profile of v0, /device:TPU:0, one launch (start us, length us, event | category | flops | bytes accessed | tf_op | source)
XLA Modules:
  0.0 109.0 jit_solution(1808363215007884239)
XLA Ops:
  7.3 0.9 reshape.112
  8.2 0.7 multiply_convert_fusion
  8.9 0.8 fusion.43
  9.8 1.9 %fusion.41 = f32[32,512]{1,0:T(8,128)} fusion(bf16[32,512]{1,0:T(8,128)(2,1)S(1)} %multiply_convert_fusion, bf16[512,512]{1,0:T(8,128)(2,1)} %param.16), kind=kOutput, calls=%fused_computation.93 | convolution fusion | flops 16777216 | bytes 622592 | tf_op jit(solution)/shard_map/dot_general | solution.py:122
  11.8 1.9 %fusion.39 = f32[32,512]{1,0:T(8,128)} fusion(bf16[32,512]{1,0:T(8,128)(2,1)S(1)} %multiply_convert_fusion, bf16[512,512]{1,0:T(8,128)(2,1)} %param.15), kind=kOutput, calls=%fused_computation.91 | convolution fusion | flops 16777216 | bytes 622592 | tf_op jit(solution)/shard_map/dot_general | solution.py:121
  14.1 0.6 dynamic-slice
  15.4 21.2 %all-reduce.3 = (f32[32,8]{1,0:T(8,128)S(1)}, f32[32]{0:T(128)S(1)}, f32[32,8]{1,0:T(8,128)S(1)}) all-reduce(f32[32,8]{1,0:T(8,128)S(1)} %fusion.40, f32[32]{0:T(128)S(1)} %reduce_sum.48, f32[32,8]{1,0:T(8,128)S(1)} %fusion.42), channel_id=4, replica_groups=mesh['dp'=4,'kv'=4,'tp'=2] {'kv'}, use_global_device_ids=true, to_apply=%region_4.0.clone | all-reduce | flops 544 | bytes 4352
  37.2 0.1 select_reduce_fusion
  37.4 0.2 reshape.107
  37.8 15.0 %reduce-scatter.6.cloned.1.call-done = f32[8,512]{1,0:T(8,128)} async-done(((f32[32,512]{1,0:T(8,128)}), f32[8,512]{1,0:T(8,128)}) %reduce-scatter.6.cloned.1.call-update) | async-done | bytes 16400 | tf_op jit(solution)/shard_map/reduce_scatter | solution.py:128
  52.8 19.7 %reduce-scatter.4.cloned.1.call-done = f32[8,512]{1,0:T(8,128)} async-done(((f32[32,512]{1,0:T(8,128)}), f32[8,512]{1,0:T(8,128)}) %reduce-scatter.4.cloned.1.call-update) | async-done | bytes 16400 | tf_op jit(solution)/shard_map/reduce_scatter | solution.py:127
  72.5 0.8 broadcast_multiply_fusion.1
  74.0 0.3 fusion.1
  74.3 0.3 slice_reduce_fusion.4
  74.7 0.5 fusion.15
  75.3 0.3 convolution_multiply_fusion.1
  75.6 0.5 fusion.18
  76.1 0.3 multiply_reduce_fusion.1
  76.8 13.1 %all_gather.3 = bf16[32,512]{1,0:T(8,128)(2,1)S(1)} all-gather(bf16[8,512]{1,0:T(8,128)(2,1)S(1)} %reshape_reshape.3), channel_id=1, replica_groups=mesh['dp'=4,'kv'=4,'tp'=2] {'kv'}, dimensions={0}, use_global_device_ids=true | all-gather | bytes 40960 | tf_op jit(solution)/shard_map/all_gather | solution.py:154
  89.9 0.2 convolution_convert_fusion
  90.2 4.0 %psum.7 = bf16[8,4,512]{2,1,0:T(4,128)(2,1)} all-reduce(bf16[8,4,512]{2,1,0:T(4,128)(2,1)S(1)} %reshape.110), channel_id=1, replica_groups=mesh['dp'=4,'kv'=4,'tp'=2] {'tp'}, use_global_device_ids=true, to_apply=%region_12.13 | all-reduce | flops 16384 | bytes 65536 | tf_op jit(solution)/shard_map/psum | solution.py:158
  94.2 3.7 %bitcast_add_fusion = f32[2,4,8,64,64]{4,3,1,2,0:T(8,128)S(1)} fusion(f32[2,8,64,64]{3,2,1,0:T(8,128)S(1)} %reshape.107, f32[2,4,8]{1,2,0:T(8,128)S(1)} %copy.108, f32[2,8,4,4]{2,3,1,0:T(4,128)S(1)} %fusion.7, f32[2,8,4,64]{3,2,1,0:T(4,128)S(1)} %copy.96, f32[2,8,4,64,1]{3,1,2,0,4:T(8,128)S(1)} %fusion.59), kind=kOutput, calls=%fused_computation | convolution fusion | flops 13123584 | bytes 1344768 | tf_op jit(solution)/shard_map/nhtj,nhjd,nhje->nhtde/dot_general | solution.py:49
  97.9 1.8 %reshape.111 = f32[2,4,8,4096]{3,1,2,0:T(4,128)} reshape(f32[2,4,8,64,64]{4,3,1,2,0:T(8,128)S(1)} %bitcast_add_fusion) | data formatting | bytes 2097152 | tf_op jit(solution)/shard_map/reshape | solution.py:94
  99.7 2.8 %copy.111 = f32[2,4,8,4096]{3,2,1,0:T(8,128)} copy(f32[2,4,8,4096]{3,1,2,0:T(4,128)} %reshape.111) | data formatting | bytes 2097152
  (70 shorter events, 2.6 us)
Async XLA Ops:
  7.2 1.8 %copy-start = (bf16[512,512]{1,0:T(8,128)(2,1)S(1)}, bf16[512,512]{1,0:T(8,128)(2,1)}, u32[]{:S(2)}) copy-start(bf16[512,512]{1,0:T(8,128)(2,1)} %param.17) | copy-start | bytes 1572868
  7.2 7.0 %copy-start.10 = (u32[32]{0:T(128)S(1)}, u32[32]{0:T(128)}, u32[]{:S(2)}) copy-start(u32[32]{0:T(128)} %constant.39) | copy-start | bytes 388
  7.2 6.5 %copy-start.3 = (bf16[8,4,512]{2,1,0:T(4,128)(2,1)S(1)}, bf16[8,4,512]{2,1,0:T(4,128)(2,1)}, u32[]{:S(2)}) copy-start(bf16[8,4,512]{2,1,0:T(4,128)(2,1)} %param.13) | copy-start | bytes 98308
  7.2 6.6 %copy-start.8 = (f32[8]{0:T(128)S(1)}, f32[8]{0:T(128)}, u32[]{:S(2)}) copy-start(f32[8]{0:T(128)} %param.20) | copy-start | bytes 100
  7.2 6.7 %copy-start.4 = (bf16[512,8]{0,1:T(8,128)(2,1)S(1)}, bf16[512,8]{0,1:T(8,128)(2,1)}, u32[]{:S(2)}) copy-start(bf16[512,8]{0,1:T(8,128)(2,1)} %param.18) | copy-start | bytes 24580
  7.2 6.8 %copy-start.5 = (bf16[512,8]{0,1:T(8,128)(2,1)S(1)}, bf16[512,8]{0,1:T(8,128)(2,1)}, u32[]{:S(2)}) copy-start(bf16[512,8]{0,1:T(8,128)(2,1)} %param.19) | copy-start | bytes 24580
  7.2 29.6 %copy-start.6 = (f32[2,4,8]{2,1,0:T(4,128)S(1)}, f32[2,4,8]{2,1,0:T(4,128)}, u32[]{:S(2)}) copy-start(f32[2,4,8]{2,1,0:T(4,128)} %param.21) | copy-start | bytes 772
  7.2 29.8 %copy-start.9 = (s32[2]{0:T(128)S(1)}, s32[2]{0:T(128)}, u32[]{:S(2)}) copy-start(s32[2]{0:T(128)} %param.22) | copy-start | bytes 28
  7.3 30.0 %copy-start.1 = (f32[2,4,8,4096]{3,2,1,0:T(8,128)S(1)}, f32[2,4,8,4096]{3,2,1,0:T(8,128)}, u32[]{:S(2)}) copy-start(f32[2,4,8,4096]{3,2,1,0:T(8,128)} %param.23) | copy-start | bytes 3145732
  7.3 30.5 %reduce-scatter.8.cloned.1.call-start = ((), (), s32[]{:S(2)}) async-start(), calls=%async_computation.5 | async-start | bytes 81920 | tf_op jit(solution)/shard_map/reduce_scatter | solution.py:129
  9.8 43.0 %reduce-scatter.6.cloned.1.call-start = ((), (), s32[]{:S(2)}) async-start(), calls=%async_computation.4 | async-start | bytes 81920 | tf_op jit(solution)/shard_map/reduce_scatter | solution.py:128
  11.7 60.8 %reduce-scatter.4.cloned.1.call-start = ((), (), s32[]{:S(2)}) async-start(), calls=%async_computation.3 | async-start | bytes 81920 | tf_op jit(solution)/shard_map/reduce_scatter | solution.py:127
  37.4 39.2 %copy-start.7 = (f32[64]{0:T(128)S(1)}, f32[64]{0:T(128)}, u32[]{:S(2)}) copy-start(f32[64]{0:T(128)} %param.24) | copy-start | bytes 772
  37.4 52.6 %copy-start.2 = (bf16[512,512]{1,0:T(8,128)(2,1)S(1)}, bf16[512,512]{1,0:T(8,128)(2,1)}, u32[]{:S(2)}) copy-start(bf16[512,512]{1,0:T(8,128)(2,1)} %param.25) | copy-start | bytes 1572868
Sparse Core Ops, SparseCore 0:
  10.9 21.9 reduce-scatter.7
  35.1 17.5 reduce-scatter.5
  55.0 17.4 reduce-scatter.3
where the time goes:
time: 109 us
  blocking collectives  38.4 us (35%)
  waiting for transfers between devices  34.8 us (32%)
  between operations  14.7 us (13%)
  matrix products  10.5 us (10%)
  local copies, waits for them, and re-layouts  7.6 us (7%)
  other arithmetic  2.91 us (3%)
    unnamed x1, blocking collectives  21.2 us
    reduce_scatter x1, waiting for transfers between devices, per_device(): lax.psum_scatter(part_query, 'kv', scatter_dimension=0, tiled=True)  19.7 us
    reduce_scatter x1, waiting for transfers between devices, per_device(): lax.psum_scatter(part_key, 'kv', scatter_dimension=0, tiled=True)  15 us
    all_gather x1, blocking collectives, per_device(): lax.all_gather(normed_rows, 'kv', axis=0, tiled=True)  13.1 us
    psum x1, blocking collectives, per_device(): lax.psum(partial_value.astype(jnp.bfloat16), 'tp').astype(jnp.float32)  4 us
    dot_general x1, matrix products, delta_block(): jnp.einsum('nhtj,nhjd,nhje->nhtde', within, key_heads, corrected, precisi...  3.68 us
    unnamed x25, local copies, waits for them, and re-layouts  3.54 us
  transfers between devices with their start and end apart: 3, of which 2 were waited for; matrix products, arithmetic and copies ran while one was open for 5% of the time, Pallas kernels for 0%

commit v1 on v0

v1 whole, which is shorter than its diff:
```python
import functools
import jax
import jax.numpy as jnp
from jax import lax
from jax.experimental import pallas as pl
from jax.experimental.pallas import tpu as pltpu
from jax.sharding import PartitionSpec as P

epsilon = 1e-06
MESH = pl.DeviceIdType.MESH
f32 = jnp.float32
bf16 = jnp.bfloat16
LANES = 128


def far_first(n):
    return sorted(range(1, n), key=lambda o: (abs(2 * o - n), o))


def near_first(n):
    return sorted(range(1, n), key=lambda o: (-abs(2 * o - n), o))


def silu(u):
    return u / (1.0 + jnp.exp(-u))


def kernel(
    n,
    ntp,
    head_size,
    tokens_hbm,
    gain_hbm,
    wq_hbm,
    wk_hbm,
    wv_hbm,
    wb_hbm,
    wd_hbm,
    rate_hbm,
    extra_hbm,
    accepted_hbm,
    prior_hbm,
    onorm_hbm,
    wo_hbm,
    mixed_ref,
    states_hbm,
    tokens_v,
    gain_v,
    w_v,
    wb_v,
    wd_v,
    rate_v,
    extra_v,
    accepted_s,
    prior_v,
    onorm_v,
    wo_v,
    x_v,
    part_v,
    aux_v,
    send_v,
    recv_v,
    recva_v,
    heads_v,
    gates_v,
    spread_v,
    expand_v,
    states_v,
    att_v,
    flat_v,
    normed_v,
    recvn_v,
    outp_v,
    recvp_v,
    load_sem,
    store_sem,
    rs_send,
    rs_recv,
    ag_send,
    ag_recv,
    tp_send,
    tp_recv,
):
    me = lax.axis_index("kv")
    my_tp = lax.axis_index("tp")
    group_seqs, steps, feature_dev = tokens_v.shape
    own_seqs, _, heads, state_len = prior_v.shape
    own_rows = own_seqs * steps
    model_width = n * feature_dev

    barrier = pltpu.get_barrier_semaphore()
    for o in far_first(n):
        pl.semaphore_signal(
            barrier, inc=1, device_id={"kv": lax.rem(me + o, n)}, device_id_type=MESH
        )
    for o in range(1, ntp):
        pl.semaphore_signal(
            barrier, inc=1, device_id={"tp": lax.rem(my_tp + o, ntp)}, device_id_type=MESH
        )

    loads = {}
    for index, (name, source, target) in enumerate((
        ("tokens", tokens_hbm, tokens_v),
        ("gain", gain_hbm, gain_v),
        ("wb", wb_hbm, wb_v),
        ("wd", wd_hbm, wd_v),
        ("q", wq_hbm, w_v.at[0]),
        ("k", wk_hbm, w_v.at[1]),
        ("v", wv_hbm, w_v.at[2]),
        ("prior", prior_hbm, prior_v),
        ("rate", rate_hbm, rate_v),
        ("extra", extra_hbm, extra_v),
        ("accepted", accepted_hbm, accepted_s),
        ("onorm", onorm_hbm, onorm_v),
        ("wo", wo_hbm, wo_v),
    )):
        loads[name] = pltpu.make_async_copy(source, target, load_sem.at[index])
        loads[name].start()

    loads["tokens"].wait()
    loads["gain"].wait()
    for s in range(group_seqs):
        x_v[s * steps:(s + 1) * steps, :] = tokens_v[s].astype(f32)
    x = x_v[...]
    squares = jnp.sum(x * x, axis=1, keepdims=True)
    scaled = (x * gain_v[...]).astype(bf16)

    contract_last = (((1,), (1,)), ((), ()))
    loads["wb"].wait()
    loads["wd"].wait()
    beta_part = lax.dot_general(scaled, wb_v[...], contract_last, preferred_element_type=f32)
    decay_part = lax.dot_general(scaled, wd_v[...], contract_last, preferred_element_type=f32)
    lane = lax.broadcasted_iota(jnp.int32, (x.shape[0], LANES), 1)
    aux_v[...] = jnp.where(lane == 2 * heads, squares, 0.0).reshape(aux_v.shape)
    aux_v[:, :, 0:heads] = beta_part.reshape(n, own_rows, heads)
    aux_v[:, :, heads:2 * heads] = decay_part.reshape(n, own_rows, heads)

    pl.semaphore_wait(barrier, n - 1 + ntp - 1)

    sends = []
    rs = {}

    def remote(source, target, send_sem, recv_sem, device):
        copy = pltpu.make_async_remote_copy(
            src_ref=source,
            dst_ref=target,
            send_sem=send_sem,
            recv_sem=recv_sem,
            device_id=device,
            device_id_type=MESH,
        )
        copy.start()
        sends.append(copy)
        return copy

    for o in far_first(n):
        target = lax.rem(me + o, n)
        rs[3, o] = remote(
            aux_v.at[target], recva_v.at[o - 1], rs_send.at[3, o - 1], rs_recv.at[3, o - 1],
            {"kv": target},
        )
    for piece, name in enumerate(("q", "k", "v")):
        loads[name].wait()
        part = jnp.dot(scaled, w_v[piece], preferred_element_type=f32)
        part = part.reshape(n, own_rows, part.shape[1])
        part_v[piece] = part
        send_v[piece] = part.astype(bf16)
        for o in far_first(n):
            target = lax.rem(me + o, n)
            rs[piece, o] = remote(
                send_v.at[piece, target], recv_v.at[piece, o - 1],
                rs_send.at[piece, o - 1], rs_recv.at[piece, o - 1], {"kv": target},
            )

    entry = lax.broadcasted_iota(jnp.int32, spread_v.shape, 0)
    column = lax.broadcasted_iota(jnp.int32, spread_v.shape, 1)
    first = lax.rem(entry, head_size) * head_size
    spread_v[...] = jnp.where(
        (column >= first) & (column < first + head_size), 1.0, 0.0
    ).astype(bf16)

    for name in ("rate", "extra", "accepted", "onorm", "prior"):
        loads[name].wait()

    aux = aux_v[me]
    for o in near_first(n):
        rs[3, o].wait_recv()
        aux = aux + recva_v[o - 1]
    inverse = lax.rsqrt(aux[:, 2 * heads:2 * heads + 1] / model_width + epsilon)
    pre = aux * inverse
    beta_pre = pre[:, 0:heads]
    decay_pre = pre[:, heads:2 * heads]
    softplus = jnp.maximum(decay_pre, 0.0) + jnp.log1p(jnp.exp(-jnp.abs(decay_pre)))
    extra = jnp.concatenate([extra_v[s] for s in range(own_seqs)], axis=0)
    gates_v[...] = jnp.zeros(gates_v.shape, f32)
    gates_v[:, 0:heads] = 1.0 / (1.0 + jnp.exp(-beta_pre))
    gates_v[:, heads:2 * heads] = jnp.exp(-rate_v[...] * softplus + extra)
    gates = gates_v[...].T

    def summed(piece):
        total = part_v[piece, me]
        for o in near_first(n):
            rs[piece, o].wait_recv()
            total = total + recv_v[piece, o - 1].astype(f32)
        value = silu(total * inverse)
        for h in range(heads):
            heads_v[piece, :, h, :] = value[:, h * head_size:(h + 1) * head_size]
        return heads_v[piece]

    def unit(value):
        return value * lax.rsqrt(jnp.sum(value * value, axis=-1, keepdims=True) + epsilon)

    tall = own_rows * heads
    for piece, scale in ((0, head_size ** -0.5), (1, 1.0)):
        value = (unit(summed(piece)) * scale).reshape(tall, head_size)
        high = value.astype(bf16)
        low = (value - high.astype(f32)).astype(bf16)
        both = jnp.concatenate([high.astype(f32), low.astype(f32)], axis=1).astype(bf16)
        expand_v[piece] = jnp.dot(both, spread_v[...], preferred_element_type=f32)
    value_heads = summed(2)

    def fold(product):
        width = product.shape[1]
        while width > LANES:
            width //= 2
            product = product[:, :width] + product[:, width:]
        return product + pltpu.roll(product, head_size, 1)

    stores = []
    for s in range(own_seqs):
        state = prior_v[s, jnp.clip(accepted_s[s] - 1, 0, steps - 1)]
        for t in range(steps):
            row = s * steps + t
            block = pl.ds(row * heads, heads)
            key_wide = expand_v[1, block, :]
            beta = gates[0:heads, row:row + 1]
            decay = gates[heads:2 * heads, row:row + 1]
            value = value_heads[row]
            value = jnp.concatenate([value] * (LANES // head_size), axis=1)
            write = beta * (value - decay * fold(key_wide * state))
            write = jnp.concatenate([write] * (state_len // LANES), axis=1)
            state = decay * state + key_wide * write
            states_v[s, t] = state
            copy = pltpu.make_async_copy(
                states_v.at[s, t], states_hbm.at[s, t], store_sem.at[row]
            )
            copy.start()
            stores.append(copy)
            attended = fold(expand_v[0, block, :] * state)
            att_v[row] = attended[:, 0:head_size]

    attended = att_v[...]
    mean = jnp.sum(attended * attended, axis=-1, keepdims=True) / head_size
    att_v[...] = attended * lax.rsqrt(mean + epsilon) * onorm_v[...].reshape(1, 1, head_size)
    for h in range(heads):
        flat_v[:, h * head_size:(h + 1) * head_size] = att_v[:, h, :]
    normed = flat_v[...].astype(bf16)
    normed_v[...] = normed

    gather = {}
    for o in far_first(n):
        gather[o] = remote(
            normed_v, recvn_v.at[o - 1], ag_send.at[o - 1], ag_recv.at[o - 1],
            {"kv": lax.rem(me + o, n)},
        )
    loads["wo"].wait()
    exchange = {}

    def project(o, rows):
        outp_v[o] = jnp.dot(rows, wo_v[...], preferred_element_type=f32).astype(bf16)
        for p in range(1, ntp):
            exchange[o, p] = remote(
                outp_v.at[o], recvp_v.at[p - 1, o], tp_send.at[p - 1, o], tp_recv.at[p - 1, o],
                {"tp": lax.rem(my_tp + p, ntp)},
            )

    order = [0] + near_first(n)
    project(0, normed)
    for o in near_first(n):
        gather[o].wait_recv()
        project(o, recvn_v[o - 1])
    for o in order:
        total = outp_v[o].astype(f32)
        for p in range(1, ntp):
            exchange[o, p].wait_recv()
            total = total + recvp_v[p - 1, o].astype(f32)
        mixed_ref[lax.rem(me - o + n, n)] = total.astype(bf16)

    for copy in sends:
        copy.wait_send()
    for copy in stores:
        copy.wait()


def per_device(n, ntp, *args):
    (
        tokens, input_norm_gain, query_projection, key_projection, value_projection,
        write_strength_weight, decay_projection, head_decay_rate, token_extra_decay,
        accepted, prior_step_states, output_norm_gain, output_projection,
    ) = args
    group_seqs, steps, feature_dev = tokens.shape
    own_seqs, _, heads, state_len = prior_step_states.shape
    own_rows = own_seqs * steps
    head_size = output_norm_gain.shape[0]
    inner = query_projection.shape[1]
    out_dev = output_projection.shape[1]
    rows = group_seqs * steps
    any_spec = pl.BlockSpec(memory_space=pl.ANY)
    dma = pltpu.SemaphoreType.DMA
    mixed, states = pl.pallas_call(
        functools.partial(kernel, n, ntp, head_size),
        out_shape=(
            jax.ShapeDtypeStruct((n, own_rows, out_dev), bf16),
            jax.ShapeDtypeStruct(prior_step_states.shape, f32),
        ),
        in_specs=[any_spec] * 13,
        out_specs=(pl.BlockSpec(memory_space=pltpu.VMEM), any_spec),
        scratch_shapes=[
            pltpu.VMEM(tokens.shape, bf16),
            pltpu.VMEM((1, feature_dev), f32),
            pltpu.VMEM((3, feature_dev, inner), bf16),
            pltpu.VMEM((heads, feature_dev), bf16),
            pltpu.VMEM((heads, feature_dev), bf16),
            pltpu.VMEM((1, heads), f32),
            pltpu.VMEM(token_extra_decay.shape, f32),
            pltpu.SMEM(accepted.shape, jnp.int32),
            pltpu.VMEM(prior_step_states.shape, f32),
            pltpu.VMEM((1, head_size), f32),
            pltpu.VMEM((inner, out_dev), bf16),
            pltpu.VMEM((rows, feature_dev), f32),
            pltpu.VMEM((3, n, own_rows, inner), f32),
            pltpu.VMEM((n, own_rows, LANES), f32),
            pltpu.VMEM((3, n, own_rows, inner), bf16),
            pltpu.VMEM((3, n - 1, own_rows, inner), bf16),
            pltpu.VMEM((n - 1, own_rows, LANES), f32),
            pltpu.VMEM((3, own_rows, heads, head_size), f32),
            pltpu.VMEM((own_rows, LANES), f32),
            pltpu.VMEM((2 * head_size, state_len), bf16),
            pltpu.VMEM((2, own_rows * heads, state_len), f32),
            pltpu.VMEM(prior_step_states.shape, f32),
            pltpu.VMEM((own_rows, heads, head_size), f32),
            pltpu.VMEM((own_rows, inner), f32),
            pltpu.VMEM((own_rows, inner), bf16),
            pltpu.VMEM((n - 1, own_rows, inner), bf16),
            pltpu.VMEM((n, own_rows, out_dev), bf16),
            pltpu.VMEM((ntp - 1, n, own_rows, out_dev), bf16),
            dma((13,)),
            dma((own_rows,)),
            dma((4, n - 1)),
            dma((4, n - 1)),
            dma((n - 1,)),
            dma((n - 1,)),
            dma((ntp - 1, n)),
            dma((ntp - 1, n)),
        ],
        compiler_params=pltpu.CompilerParams(collective_id=0, has_side_effects=True),
    )(
        tokens, input_norm_gain.reshape(1, feature_dev), query_projection, key_projection,
        value_projection, write_strength_weight.T, decay_projection.T,
        head_decay_rate.reshape(1, heads), token_extra_decay, accepted, prior_step_states,
        output_norm_gain.reshape(1, head_size), output_projection,
    )
    return mixed.reshape(group_seqs, steps, out_dev), states


def solution(mesh):
    in_specs = (
        P("dp", None, "kv"),
        P("kv"),
        P("kv", "tp"),
        P("kv", "tp"),
        P("kv", "tp"),
        P("kv", "tp"),
        P("kv", "tp"),
        P("tp"),
        P(("dp", "kv"), None, "tp"),
        P(("dp", "kv")),
        P(("dp", "kv"), None, "tp", None),
        P(),
        P("tp", "kv"),
    )
    out_specs = (P("dp", None, "kv"), P(("dp", "kv"), None, "tp", None))
    body = functools.partial(per_device, mesh.shape["kv"], mesh.shape["tp"])
    return jax.shard_map(
        body, mesh=mesh, in_specs=in_specs, out_specs=out_specs, check_vma=False
    )
```

time: 109 us -> 21.8 us (0.20)
  blocking collectives: 38.4 us -> 0 us
  waiting for transfers between devices: 34.8 us -> 0 us
  Pallas kernels: 0 us -> 17.3 us
  between operations: 14.7 us -> 0.64 us
  matrix products: 10.5 us -> 0 us
  local copies, waits for them, and re-layouts: 7.6 us -> 3.66 us
  other arithmetic: 2.91 us -> 0 us
    reduce_scatter x3 -> x0, waiting for transfers between devices: 34.7 us -> none  [the longest x1 19.7 us: per_device(): lax.psum_scatter(part_query, 'kv', scatter_dimension=0, tiled=True)]
    unnamed x1 -> x0, blocking collectives: 21.2 us -> none
    pallas_call x0 -> x1, Pallas kernels: none -> 17.3 us  [per_device(): pl.pallas_call(functools.partial(kernel, n, ntp, head_size), out_shape=(j...]
    all_gather x1 -> x0, blocking collectives: 13.1 us -> none  [per_device(): lax.all_gather(normed_rows, 'kv', axis=0, tiled=True)]
    dot_general x12 -> x0, matrix products: 10.5 us -> none  [the longest x1 3.68 us: delta_block(): jnp.einsum('nhtj,nhjd,nhje->nhtde', within, key_heads, corrected, precisi...]
    psum x1 -> x0, blocking collectives: 4 us -> none  [per_device(): lax.psum(partial_value.astype(jnp.bfloat16), 'tp').astype(jnp.float32)]
    unnamed x25 -> x1, local copies, waits for them, and re-layouts: 3.54 us -> 2.27 us
    reshape x6 -> x1, local copies, waits for them, and re-layouts: 2.31 us -> 1.39 us  [per_device(): return (mixed.reshape(group_seqs, steps, out_dev), states)]
  transfers between devices with their start and end apart: 3 -> 0, of which waited for: 2 -> 0; matrix products, arithmetic and copies ran while one was open for 5% -> 0% of each run, Pallas kernels for 0% -> 0%
where the time goes in v1:
time: 21.8 us; the launch traced here: 21.6 us
  Pallas kernels  17.3 us (79%)
  local copies, waits for them, and re-layouts  3.66 us (17%)
  between operations  0.64 us (3%)
    pallas_call x1, Pallas kernels, per_device(): pl.pallas_call(functools.partial(kernel, n, ntp, head_size), out_shape=(j...  17.3 us
    unnamed x1, local copies, waits for them, and re-layouts  2.27 us
    reshape x1, local copies, waits for them, and re-layouts, per_device(): return (mixed.reshape(group_seqs, steps, out_dev), states)  1.39 us

profile of v1, /device:TPU:0, one launch (start us, length us, event | category | flops | bytes accessed | tf_op | source)
XLA Modules:
  0.0 21.6 jit_solution(11695330514258805403)
XLA Ops:
  0.6 17.3 %shard_map.140 = (bf16[4,8,512]{2,1,0:T(8,128)(2,1)}, f32[2,4,8,4096]{3,2,1,0:T(8,128)}) custom-call(bf16[8,4,512]{2,1,0:T(4,128)(2,1)} %tokens_hbm.1, f32[1,512]{1,0:T(1,128)} %bitcast.7, bf16[512,512]{1,0:T(8,128)(2,1)} %wq_hbm.1, bf16[512,512]{1,0:T(8,128)(2,1)} %wk_hbm.1, bf16[512,512]{1,0:T(8,128)(2,1)} %wv_hbm.1, bf16[8,512]{1,0:T(8,128)(2,1)} %bitcast.5, ...), custom_call_target="tpu_custom_call" | custom-call | tf_op jit(solution)/shard_map/pallas_call | solution.py:310
  17.9 1.4 %reshape.19 = bf16[8,4,512]{2,1,0:T(4,128)(2,1)} reshape(bf16[4,8,512]{2,1,0:T(8,128)(2,1)} %get-tuple-element.4) | data formatting | bytes 65536 | tf_op jit(solution)/shard_map/reshape | solution.py:363
  19.3 2.3 %copy.16 = f32[2,4,8,4096]{3,2,1,0:T(8,128)} copy(f32[2,4,8,4096]{3,2,1,0:T(8,128)} %get-tuple-element.9) | data formatting | bytes 2097152

commit v2 on v1

--- a/solution.py
+++ b/solution.py
@@ -11,6 +11,7 @@
 f32 = jnp.float32
 bf16 = jnp.bfloat16
 LANES = 128
+VMEM_LIMIT = 32 * 2 ** 20
 
 
 def far_first(n):
@@ -43,7 +44,7 @@
     onorm_hbm,
     wo_hbm,
     mixed_ref,
-    states_hbm,
+    states_v,
     tokens_v,
     gain_v,
     w_v,
@@ -65,7 +66,6 @@
     gates_v,
     spread_v,
     expand_v,
-    states_v,
     att_v,
     flat_v,
     normed_v,
@@ -73,7 +73,6 @@
     outp_v,
     recvp_v,
     load_sem,
-    store_sem,
     rs_send,
     rs_recv,
     ag_send,
@@ -174,7 +173,7 @@
 
     entry = lax.broadcasted_iota(jnp.int32, spread_v.shape, 0)
     column = lax.broadcasted_iota(jnp.int32, spread_v.shape, 1)
-    first = lax.rem(entry, head_size) * head_size
+    first = jnp.where(entry < head_size, entry, entry - head_size) * head_size
     spread_v[...] = jnp.where(
         (column >= first) & (column < first + head_size), 1.0, 0.0
     ).astype(bf16)
@@ -226,7 +225,6 @@
             product = product[:, :width] + product[:, width:]
         return product + pltpu.roll(product, head_size, 1)
 
-    stores = []
     for s in range(own_seqs):
         state = prior_v[s, jnp.clip(accepted_s[s] - 1, 0, steps - 1)]
         for t in range(steps):
@@ -241,11 +239,6 @@
             write = jnp.concatenate([write] * (state_len // LANES), axis=1)
             state = decay * state + key_wide * write
             states_v[s, t] = state
-            copy = pltpu.make_async_copy(
-                states_v.at[s, t], states_hbm.at[s, t], store_sem.at[row]
-            )
-            copy.start()
-            stores.append(copy)
             attended = fold(expand_v[0, block, :] * state)
             att_v[row] = attended[:, 0:head_size]
 
@@ -284,11 +277,22 @@
         for p in range(1, ntp):
             exchange[o, p].wait_recv()
             total = total + recvp_v[p - 1, o].astype(f32)
-        mixed_ref[lax.rem(me - o + n, n)] = total.astype(bf16)
+        source = lax.rem(me - o + n, n) * own_seqs
+        for s in range(own_seqs):
+            mixed_ref[source + s] = total[s * steps:(s + 1) * steps].astype(bf16)
 
     for copy in sends:
         copy.wait_send()
-    for copy in stores:
+
+
+def finish(mixed_v, states_v, mixed_hbm, states_hbm, sem):
+    copies = (
+        pltpu.make_async_copy(states_v, states_hbm, sem.at[0]),
+        pltpu.make_async_copy(mixed_v, mixed_hbm, sem.at[1]),
+    )
+    for copy in copies:
+        copy.start()
+    for copy in copies:
         copy.wait()
 
 
@@ -306,15 +310,20 @@
     out_dev = output_projection.shape[1]
     rows = group_seqs * steps
     any_spec = pl.BlockSpec(memory_space=pl.ANY)
+    vmem_spec = pl.BlockSpec(memory_space=pltpu.VMEM)
     dma = pltpu.SemaphoreType.DMA
+
+    def hbm(array):
+        return pltpu.with_memory_space_constraint(array, pltpu.HBM)
+
     mixed, states = pl.pallas_call(
         functools.partial(kernel, n, ntp, head_size),
         out_shape=(
-            jax.ShapeDtypeStruct((n, own_rows, out_dev), bf16),
-            jax.ShapeDtypeStruct(prior_step_states.shape, f32),
+            pltpu.VMEM((group_seqs, steps, out_dev), bf16),
+            pltpu.VMEM(prior_step_states.shape, f32),
         ),
         in_specs=[any_spec] * 13,
-        out_specs=(pl.BlockSpec(memory_space=pltpu.VMEM), any_spec),
+        out_specs=(vmem_spec, vmem_spec),
         scratch_shapes=[
             pltpu.VMEM(tokens.shape, bf16),
             pltpu.VMEM((1, feature_dev), f32),
@@ -337,7 +346,6 @@
             pltpu.VMEM((own_rows, LANES), f32),
             pltpu.VMEM((2 * head_size, state_len), bf16),
             pltpu.VMEM((2, own_rows * heads, state_len), f32),
-            pltpu.VMEM(prior_step_states.shape, f32),
             pltpu.VMEM((own_rows, heads, head_size), f32),
             pltpu.VMEM((own_rows, inner), f32),
             pltpu.VMEM((own_rows, inner), bf16),
@@ -345,7 +353,6 @@
             pltpu.VMEM((n, own_rows, out_dev), bf16),
             pltpu.VMEM((ntp - 1, n, own_rows, out_dev), bf16),
             dma((13,)),
-            dma((own_rows,)),
             dma((4, n - 1)),
             dma((4, n - 1)),
             dma((n - 1,)),
@@ -353,14 +360,26 @@
             dma((ntp - 1, n)),
             dma((ntp - 1, n)),
         ],
-        compiler_params=pltpu.CompilerParams(collective_id=0, has_side_effects=True),
-    )(
+        compiler_params=pltpu.CompilerParams(
+            collective_id=0, has_side_effects=True, vmem_limit_bytes=VMEM_LIMIT
+        ),
+    )(*map(hbm, (
         tokens, input_norm_gain.reshape(1, feature_dev), query_projection, key_projection,
         value_projection, write_strength_weight.T, decay_projection.T,
         head_decay_rate.reshape(1, heads), token_extra_decay, accepted, prior_step_states,
         output_norm_gain.reshape(1, head_size), output_projection,
-    )
-    return mixed.reshape(group_seqs, steps, out_dev), states
+    )))
+    return pl.pallas_call(
+        finish,
+        out_shape=(
+            jax.ShapeDtypeStruct(mixed.shape, bf16),
+            jax.ShapeDtypeStruct(states.shape, f32),
+        ),
+        in_specs=[vmem_spec, vmem_spec],
+        out_specs=(any_spec, any_spec),
+        scratch_shapes=[dma((2,))],
+        compiler_params=pltpu.CompilerParams(vmem_limit_bytes=VMEM_LIMIT // 4),
+    )(mixed, states)
 
 
 def solution(mesh):

time: 21.8 us -> 18.3 us (0.84)
  local copies, waits for them, and re-layouts: 3.66 us -> 0 us
    unnamed x1 -> x0, local copies, waits for them, and re-layouts: 2.27 us -> none
    reshape x1 -> x0, local copies, waits for them, and re-layouts: 1.39 us -> none  [per_device(): return (mixed.reshape(group_seqs, steps, out_dev), states)]
    pallas_call x1 -> x2, Pallas kernels: 17.3 us -> 17.5 us  [the longest x1 16.5 us: per_device(): pl.pallas_call(functools.partial(kernel, n, ntp, head_size), out_shape=(p...]
where the time goes in v2:
time: 18.3 us; the launch traced here: 18.2 us
  Pallas kernels  17.5 us (96%)
  between operations  0.64 us (3%)
    pallas_call x1, Pallas kernels, per_device(): pl.pallas_call(functools.partial(kernel, n, ntp, head_size), out_shape=(p...  16.5 us
    pallas_call x1, Pallas kernels, per_device(): pl.pallas_call(finish, out_shape=(jax.ShapeDtypeStruct(mixed.shape, bf16)...  0.99 us

profile of v2, /device:TPU:0, one launch (start us, length us, event | category | flops | bytes accessed | tf_op | source)
XLA Modules:
  0.0 18.2 jit_solution(17038999742264226942)
XLA Ops:
  0.6 16.5 %shard_map.140 = (bf16[8,4,512]{2,1,0:T(4,128)(2,1)S(1)}, f32[2,4,8,4096]{3,2,1,0:T(8,128)S(1)}) custom-call(bf16[8,4,512]{2,1,0:T(4,128)(2,1)} %tokens_hbm.1, f32[1,512]{1,0:T(1,128)} %bitcast.7, bf16[512,512]{1,0:T(8,128)(2,1)} %wq_hbm.1, bf16[512,512]{1,0:T(8,128)(2,1)} %wk_hbm.1, bf16[512,512]{1,0:T(8,128)(2,1)} %wv_hbm.1, bf16[8,512]{1,0:T(8,128)(2,1)} %bitcast.5, ...), custom_call_target="tpu_custom_call" | custom-call | tf_op jit(solution)/shard_map/pallas_call | solution.py:319
  17.2 1.0 %shard_map.141 = (bf16[8,4,512]{2,1,0:T(4,128)(2,1)}, f32[2,4,8,4096]{3,2,1,0:T(8,128)}) custom-call(bf16[8,4,512]{2,1,0:T(4,128)(2,1)S(1)} %get-tuple-element.4.mixed_v, f32[2,4,8,4096]{3,2,1,0:T(8,128)S(1)} %get-tuple-element.5.states_v), custom_call_target="tpu_custom_call" | custom-call | tf_op jit(solution)/shard_map/pallas_call | solution.py:372

commit v3 on v2

--- a/solution.py
+++ b/solution.py
@@ -134,6 +134,14 @@
     aux_v[:, :, 0:heads] = beta_part.reshape(n, own_rows, heads)
     aux_v[:, :, heads:2 * heads] = decay_part.reshape(n, own_rows, heads)
 
+    def project_in(piece, name):
+        loads[name].wait()
+        part = jnp.dot(scaled, w_v[piece], preferred_element_type=f32)
+        part = part.reshape(n, own_rows, part.shape[1])
+        part_v[piece] = part
+        send_v[piece] = part.astype(bf16)
+
+    project_in(0, "q")
     pl.semaphore_wait(barrier, n - 1 + ntp - 1)
 
     sends = []
@@ -159,11 +167,8 @@
             {"kv": target},
         )
     for piece, name in enumerate(("q", "k", "v")):
-        loads[name].wait()
-        part = jnp.dot(scaled, w_v[piece], preferred_element_type=f32)
-        part = part.reshape(n, own_rows, part.shape[1])
-        part_v[piece] = part
-        send_v[piece] = part.astype(bf16)
+        if piece > 0:
+            project_in(piece, name)
         for o in far_first(n):
             target = lax.rem(me + o, n)
             rs[piece, o] = remote(
@@ -225,9 +230,12 @@
             product = product[:, :width] + product[:, width:]
         return product + pltpu.roll(product, head_size, 1)
 
-    for s in range(own_seqs):
-        state = prior_v[s, jnp.clip(accepted_s[s] - 1, 0, steps - 1)]
-        for t in range(steps):
+    current = [
+        prior_v[s, jnp.clip(accepted_s[s] - 1, 0, steps - 1)] for s in range(own_seqs)
+    ]
+    for t in range(steps):
+        for s in range(own_seqs):
+            state = current[s]
             row = s * steps + t
             block = pl.ds(row * heads, heads)
             key_wide = expand_v[1, block, :]
@@ -239,6 +247,7 @@
             write = jnp.concatenate([write] * (state_len // LANES), axis=1)
             state = decay * state + key_wide * write
             states_v[s, t] = state
+            current[s] = state
             attended = fold(expand_v[0, block, :] * state)
             att_v[row] = attended[:, 0:head_size]
 
@@ -286,10 +295,15 @@
 
 
 def finish(mixed_v, states_v, mixed_hbm, states_hbm, sem):
-    copies = (
-        pltpu.make_async_copy(states_v, states_hbm, sem.at[0]),
-        pltpu.make_async_copy(mixed_v, mixed_hbm, sem.at[1]),
-    )
+    own_seqs, steps = states_v.shape[:2]
+    copies = [
+        pltpu.make_async_copy(
+            states_v.at[s, t], states_hbm.at[s, t], sem.at[1 + s * steps + t]
+        )
+        for s in range(own_seqs)
+        for t in range(steps)
+    ]
+    copies.append(pltpu.make_async_copy(mixed_v, mixed_hbm, sem.at[0]))
     for copy in copies:
         copy.start()
     for copy in copies:
@@ -377,7 +391,7 @@
         ),
         in_specs=[vmem_spec, vmem_spec],
         out_specs=(any_spec, any_spec),
-        scratch_shapes=[dma((2,))],
+        scratch_shapes=[dma((1 + own_rows,))],
         compiler_params=pltpu.CompilerParams(vmem_limit_bytes=VMEM_LIMIT // 4),
     )(mixed, states)
 

time: 18.3 us -> 18.4 us (level)
  no operation moved by 1% of the time
where the time goes in v3:
time: 18.4 us; the launch traced here: 18.2 us
  Pallas kernels  17.6 us (96%)
  between operations  0.64 us (3%)
    pallas_call x1, Pallas kernels, per_device(): pl.pallas_call(functools.partial(kernel, n, ntp, head_size), out_shape=(p...  16.5 us
    pallas_call x1, Pallas kernels, per_device(): pl.pallas_call(finish, out_shape=(jax.ShapeDtypeStruct(mixed.shape, bf16)...  1.04 us

profile of v3, /device:TPU:0, one launch (start us, length us, event | category | flops | bytes accessed | tf_op | source)
XLA Modules:
  0.0 18.2 jit_solution(11713423880002252608)
XLA Ops:
  0.6 16.5 %shard_map.140 = (bf16[8,4,512]{2,1,0:T(4,128)(2,1)S(1)}, f32[2,4,8,4096]{3,2,1,0:T(8,128)S(1)}) custom-call(bf16[8,4,512]{2,1,0:T(4,128)(2,1)} %tokens_hbm.1, f32[1,512]{1,0:T(1,128)} %bitcast.7, bf16[512,512]{1,0:T(8,128)(2,1)} %wq_hbm.1, bf16[512,512]{1,0:T(8,128)(2,1)} %wk_hbm.1, bf16[512,512]{1,0:T(8,128)(2,1)} %wv_hbm.1, bf16[8,512]{1,0:T(8,128)(2,1)} %bitcast.5, ...), custom_call_target="tpu_custom_call" | custom-call | tf_op jit(solution)/shard_map/pallas_call | solution.py:333
  17.2 1.0 %shard_map.141 = (bf16[8,4,512]{2,1,0:T(4,128)(2,1)}, f32[2,4,8,4096]{3,2,1,0:T(8,128)}) custom-call(bf16[8,4,512]{2,1,0:T(4,128)(2,1)S(1)} %get-tuple-element.4.mixed_v, f32[2,4,8,4096]{3,2,1,0:T(8,128)S(1)} %get-tuple-element.5.states_v), custom_call_target="tpu_custom_call" | custom-call | tf_op jit(solution)/shard_map/pallas_call | solution.py:386

commit v4 on v3

--- a/solution.py
+++ b/solution.py
@@ -139,7 +139,7 @@
         part = jnp.dot(scaled, w_v[piece], preferred_element_type=f32)
         part = part.reshape(n, own_rows, part.shape[1])
         part_v[piece] = part
-        send_v[piece] = part.astype(bf16)
+        send_v[:, piece] = part.astype(bf16)
 
     project_in(0, "q")
     pl.semaphore_wait(barrier, n - 1 + ntp - 1)
@@ -166,13 +166,14 @@
             aux_v.at[target], recva_v.at[o - 1], rs_send.at[3, o - 1], rs_recv.at[3, o - 1],
             {"kv": target},
         )
-    for piece, name in enumerate(("q", "k", "v")):
+    for piece, span in ((0, pl.ds(0, 1)), (1, pl.ds(1, 2))):
         if piece > 0:
-            project_in(piece, name)
+            project_in(1, "k")
+            project_in(2, "v")
         for o in far_first(n):
             target = lax.rem(me + o, n)
             rs[piece, o] = remote(
-                send_v.at[piece, target], recv_v.at[piece, o - 1],
+                send_v.at[target, span], recv_v.at[o - 1, span],
                 rs_send.at[piece, o - 1], rs_recv.at[piece, o - 1], {"kv": target},
             )
 
@@ -204,8 +205,9 @@
     def summed(piece):
         total = part_v[piece, me]
         for o in near_first(n):
-            rs[piece, o].wait_recv()
-            total = total + recv_v[piece, o - 1].astype(f32)
+            if piece < 2:
+                rs[piece, o].wait_recv()
+            total = total + recv_v[o - 1, piece].astype(f32)
         value = silu(total * inverse)
         for h in range(heads):
             heads_v[piece, :, h, :] = value[:, h * head_size:(h + 1) * head_size]
@@ -353,8 +355,8 @@
             pltpu.VMEM((rows, feature_dev), f32),
             pltpu.VMEM((3, n, own_rows, inner), f32),
             pltpu.VMEM((n, own_rows, LANES), f32),
-            pltpu.VMEM((3, n, own_rows, inner), bf16),
-            pltpu.VMEM((3, n - 1, own_rows, inner), bf16),
+            pltpu.VMEM((n, 3, own_rows, inner), bf16),
+            pltpu.VMEM((n - 1, 3, own_rows, inner), bf16),
             pltpu.VMEM((n - 1, own_rows, LANES), f32),
             pltpu.VMEM((3, own_rows, heads, head_size), f32),
             pltpu.VMEM((own_rows, LANES), f32),

time: 18.4 us -> 18.3 us (level)
  no operation moved by 1% of the time
where the time goes in v4:
time: 18.3 us; the launch traced here: 18.1 us
  Pallas kernels  17.5 us (96%)
  between operations  0.64 us (3%)
    pallas_call x1, Pallas kernels, per_device(): pl.pallas_call(functools.partial(kernel, n, ntp, head_size), out_shape=(p...  16.4 us
    pallas_call x1, Pallas kernels, per_device(): pl.pallas_call(finish, out_shape=(jax.ShapeDtypeStruct(mixed.shape, bf16)...  1.04 us

profile of v4, /device:TPU:0, one launch (start us, length us, event | category | flops | bytes accessed | tf_op | source)
XLA Modules:
  0.0 18.1 jit_solution(4904897217136821980)
XLA Ops:
  0.6 16.4 %shard_map.140 = (bf16[8,4,512]{2,1,0:T(4,128)(2,1)S(1)}, f32[2,4,8,4096]{3,2,1,0:T(8,128)S(1)}) custom-call(bf16[8,4,512]{2,1,0:T(4,128)(2,1)} %tokens_hbm.1, f32[1,512]{1,0:T(1,128)} %bitcast.7, bf16[512,512]{1,0:T(8,128)(2,1)} %wq_hbm.1, bf16[512,512]{1,0:T(8,128)(2,1)} %wk_hbm.1, bf16[512,512]{1,0:T(8,128)(2,1)} %wv_hbm.1, bf16[8,512]{1,0:T(8,128)(2,1)} %bitcast.5, ...), custom_call_target="tpu_custom_call" | custom-call | tf_op jit(solution)/shard_map/pallas_call | solution.py:335
  17.1 1.0 %shard_map.141 = (bf16[8,4,512]{2,1,0:T(4,128)(2,1)}, f32[2,4,8,4096]{3,2,1,0:T(8,128)}) custom-call(bf16[8,4,512]{2,1,0:T(4,128)(2,1)S(1)} %get-tuple-element.4.mixed_v, f32[2,4,8,4096]{3,2,1,0:T(8,128)S(1)} %get-tuple-element.5.states_v), custom_call_target="tpu_custom_call" | custom-call | tf_op jit(solution)/shard_map/pallas_call | solution.py:388
